TPU v7x, 32 devices: a whole 2x2x4 slice. The times are simulated.
32 devices in a mesh: ep: 4 (over y, x), tp: 8 (over z, core).
Axes of the slice: x: 2, y: 2, z: 4, core: 2. Of those that a mesh axis runs over, the one named last changes fastest.
Arguments:
- tokens: bfloat16 [256, 2048], P('ep', 'tp'), may hold values from -6 to 6
- norm_gain: float32 [2048], replicated, may hold values from 0.5 to 1.5
- group_pick: int32 [256, 1], P('ep'), may hold values from 0 to 3; in each aligned block of 64 rows (0 to 63, 64 to 127, ...) at most 64 rows name the same one
- inner_pick: int32 [256, 2], P('ep'), may hold values from 0 to 3, all different within a row
- route_weight: float32 [256, 2], P('ep'), may hold values from 0.3 to 1
- w_gate: bfloat16 [16, 1024, 2048], P('ep', 'tp'), may hold values from -0.125 to 0.125
- w_up: bfloat16 [16, 1024, 2048], P('ep', 'tp'), may hold values from -0.125 to 0.125
- w_down: bfloat16 [16, 1024, 2048], P('ep', 'tp'), may hold values from -0.1875 to 0.1875
Outputs:
- mixed: bfloat16 [256, 2048], P('ep', 'tp')
Inputs may be any that keep to these rules, and one draw needn't show every extreme that they name: `group_pick`: every entry is a group, 0 to 3; among the 64 tokens of any one index of ep no group is chosen more than 64 times, a bound that some block reaches. `inner_pick`: each row names 2 different experts of the chosen group, each 0 to 3.
All inputs are finite; a program needn't handle non-finite values.
Results may differ from a plain program's by a relative error of at most 0.002.
Values may be sent and summed in bfloat16 or wider, within the bound.
A program may use at most 64 MiB of HBM per device.

v0:
```python
import jax
import jax.numpy as jnp
from jax import lax
from jax.sharding import PartitionSpec as P

epsilon = 1e-06


def scattered(portion, rows, axis):
    count = rows * lax.axis_size(axis)
    return lax.psum_scatter(portion(jnp.int32(0), count), axis, scatter_dimension=0, tiled=True)


def rms_normed(rows, norm_gain):
    widened = rows.astype(jnp.float32)
    scaled = lax.rsqrt(jnp.mean(widened * widened, axis=-1, keepdims=True) + epsilon)
    return (widened * scaled * norm_gain).astype(jnp.bfloat16)


def per_device(tokens, norm_gain, group_pick, inner_pick, route_weight, w_gate, w_up, w_down):
    ep_size = lax.axis_size("ep")
    tok_rows = tokens.shape[0]
    feature_share = tokens.shape[1]
    inner_count = w_gate.shape[0]
    capacity = min(tok_rows, 4 * tok_rows // ep_size + 2)
    slot_count = ep_size * capacity
    groups = group_pick[:, 0]
    member = (groups[:, None] == jnp.arange(ep_size, dtype=jnp.int32)[None, :]).astype(jnp.int32)
    earlier = jnp.sum((jnp.cumsum(member, axis=0) - member) * member, axis=1)
    position = (groups * capacity + earlier).astype(jnp.int32)
    placing = position[None, :] == jnp.arange(slot_count, dtype=jnp.int32)[:, None]
    local_gates = jnp.sum(
        jax.nn.one_hot(inner_pick, inner_count, dtype=jnp.float32) * route_weight[:, :, None],
        axis=1,
    )
    packed_rows = jnp.dot(
        placing.astype(jnp.bfloat16), tokens, preferred_element_type=jnp.float32
    ).astype(jnp.bfloat16)
    packed_gates = jnp.dot(
        placing.astype(jnp.float32), local_gates, precision=lax.Precision.HIGHEST
    )
    packed_rows = packed_rows.reshape(ep_size, capacity, feature_share)
    packed_gates = packed_gates.reshape(ep_size, capacity, inner_count)
    arrived_rows = lax.all_to_all(packed_rows, "ep", split_axis=0, concat_axis=0, tiled=True)
    arrived_gates = lax.all_to_all(packed_gates, "ep", split_axis=0, concat_axis=0, tiled=True)
    full_rows = lax.all_gather(arrived_rows, "tp", axis=2, tiled=True).reshape(slot_count, -1)
    normed = rms_normed(full_rows, norm_gain)
    gate_proj = jnp.einsum("sd,efd->esf", normed, w_gate, preferred_element_type=jnp.float32)
    up_proj = jnp.einsum("sd,efd->esf", normed, w_up, preferred_element_type=jnp.float32)
    hidden = (jax.nn.silu(gate_proj) * up_proj).astype(jnp.bfloat16)
    slot_gates = jnp.transpose(arrived_gates.reshape(slot_count, inner_count))

    def weighted_sum(down_part):
        products = jnp.einsum("esf,efd->esd", hidden, down_part, preferred_element_type=jnp.float32)
        return jnp.sum(slot_gates[:, :, None] * products, axis=0)

    def column_term(first_row, row_count):
        down_part = lax.dynamic_slice_in_dim(w_down, first_row, row_count, 2)
        return jnp.transpose(weighted_sum(down_part))

    own_share = scattered(column_term, feature_share, "tp")
    partial_rows = jnp.transpose(own_share).reshape(ep_size, capacity, feature_share)
    returned = (
        lax.all_to_all(
            partial_rows.astype(jnp.bfloat16), "ep", split_axis=0, concat_axis=0, tiled=True
        )
        .astype(partial_rows.dtype)
        .reshape(slot_count, feature_share)
    )
    mixed_rows = jnp.take(returned, position, axis=0)
    return mixed_rows.astype(jnp.bfloat16)


def solution(mesh):
    return jax.shard_map(
        per_device,
        mesh=mesh,
        in_specs=(
            P("ep", "tp"),
            P(),
            P("ep", None),
            P("ep", None),
            P("ep", None),
            P("ep", "tp", None),
            P("ep", "tp", None),
            P("ep", "tp", None),
        ),
        out_specs=P("ep", "tp"),
        check_vma=False,
    )
```

profile of v0, /device:TPU:0, one launch (start us, length us, event | category | flops | bytes accessed | tf_op | source)
XLA Modules:
  0.0 108.2 jit_solution(1318259087048628274)
XLA Ops:
  6.5 0.0 copy-start
  6.5 0.0 all-gather.2.cloned.1.call-start
  6.5 0.9 fusion.19
  7.4 0.1 reduce_window_sum.11
  7.5 0.8 select_reduce_fusion
  8.4 0.7 multiply_add_fusion.1
  9.0 0.9 convolution_convert_fusion
  9.9 10.2 %all_to_all.15 = bf16[4,64,256]{2,1,0:T(8,128)(2,1)} all-to-all(bf16[4,64,256]{2,1,0:T(8,128)(2,1)S(1)} %bitcast.59), channel_id=1, replica_groups=mesh['ep'=4,'tp'=8] {'ep'}, dimensions={0} | all-to-all | bytes 262144 | tf_op jit(solution)/shard_map/all_to_all | solution.py:44
  20.1 0.0 all-gather.2.cloned.1.call-update
  20.1 0.0 reduce-scatter.2.cloned.1.call-start
  20.2 0.7 select_reduce_fusion.1
  20.9 0.3 fusion.22
  21.2 0.1 reshape.85
  21.3 7.0 %all_to_all.16 = f32[4,1,256]{2,1,0:T(1,128)S(1)} all-to-all(f32[4,1,256]{2,1,0:T(1,128)S(1)} %reshape.85), channel_id=1, replica_groups=mesh['ep'=4,'tp'=8] {'ep'}, dimensions={0} | all-to-all | bytes 8192 | tf_op jit(solution)/shard_map/all_to_all | solution.py:45
  28.3 0.5 broadcast.59
  28.8 0.7 reduce.1
  29.5 0.1 reshape.86
  29.6 0.1 reshape.68
  29.7 15.2 %all-gather.2.cloned.1.call-done = bf16[4,64,2048]{2,1,0:T(8,128)(2,1)} async-done(((bf16[4,64,256]{2,1,0:T(8,128)(2,1)}), bf16[4,64,2048]{2,1,0:T(8,128)(2,1)}) %all-gather.2.cloned.1.call-update) | async-done | bytes 1048592 | tf_op jit(solution)/shard_map/all_gather | solution.py:46
  44.8 1.5 %multiply_reduce_fusion.1 = f32[4,64]{1,0:T(4,128)S(1)} fusion(bf16[4,64,2048]{2,1,0:T(8,128)(2,1)} %all-gather.2.cloned.1.call-done), kind=kLoop, calls=%fused_computation.5 | loop fusion | flops 1572608 | bytes 1049600 | tf_op jit(solution)/shard_map/reduce_sum | solution.py:16
  46.4 0.1 rsqrt.12
  46.5 0.0 copy-start.2
  46.5 1.7 %fusion.1 = bf16[256,2048]{1,0:T(8,128)(2,1)S(1)} fusion(f32[2048]{0:T(1024)} %param.9, f32[256]{0:T(256)S(1)} %rsqrt.12, bf16[4,64,2048]{2,1,0:T(8,128)(2,1)} %all-gather.2.cloned.1.call-done), kind=kLoop, calls=%fused_computation.4 | loop fusion | flops 2097152 | bytes 2106368 | tf_op jit(solution)/shard_map/convert_element_type | solution.py:17
  48.2 0.2 copy-done.2
  48.4 1.6 %convolution_bitcast_fusion.1 = f32[4,256,128]{2,1,0:T(8,128)} fusion(bf16[4,128,2048]{2,1,0:T(8,128)(2,1)S(1)} %copy-done.2, bf16[256,2048]{1,0:T(8,128)(2,1)S(1)} %fusion.1), kind=kOutput, calls=%fused_computation.8 | convolution fusion | flops 536870912 | bytes 3670016 | tf_op jit(solution)/shard_map/sd,efd->esf/dot_general | solution.py:48
  49.9 0.0 copy-done
  49.9 5.3 %multiply_reduce_fusion = f32[256,2048]{1,0:T(8,128)} fusion(bf16[4,128,2048]{2,1,0:T(8,128)(2,1)S(1)} %copy-done, f32[4,256]{1,0:T(4,128)S(1)} %bitcast.63, bf16[4,128,2048]{2,1,0:T(8,128)(2,1)} %param.14, bf16[256,2048]{1,0:T(8,128)(2,1)S(1)} %fusion.1, f32[4,256,128]{2,1,0:T(8,128)} %convolution_bitcast_fusion.1), kind=kOutput, calls=%fused_computation.1 | convolution fusion | flops 1078198272 | bytes 7868416 | tf_op jit(solution)/shard_map/esf,efd->esd/dot_general | solution.py:54
  55.2 0.0 copy-start.1
  55.2 0.0 reduce-scatter.2.cloned.1.call-update
  55.3 0.6 copy-done.1
  55.9 33.3 %reduce-scatter.2.cloned.1.call-done = f32[256,256]{0,1:T(8,128)} async-done(((f32[2048,256]{0,1:T(8,128)}), f32[256,256]{0,1:T(8,128)}) %reduce-scatter.2.cloned.1.call-update) | async-done | bytes 262160 | tf_op jit(solution)/shard_map/reduce_scatter | solution.py:11
  89.2 1.6 %convert_element_type.45 = bf16[256,256]{0,1:T(8,128)(2,1)} convert(f32[256,256]{0,1:T(8,128)} %reduce-scatter.2.cloned.1.call-done) | non-fusion elementwise | flops 65536 | bytes 393216 | tf_op jit(solution)/shard_map/convert_element_type | solution.py:65
  90.8 4.1 %all-to-all-start.2 = ((bf16[4,64,256]{2,1,0:T(8,128)(2,1)}), bf16[4,64,256]{2,1,0:T(8,128)(2,1)S(1)}, u32[]{:S(2)}, u32[]{:S(2)}) async-start(bf16[4,64,256]{2,1,0:T(8,128)(2,1)} %bitcast.12), calls=%async_computation.3 | async-start | bytes 262144 | tf_op jit(solution)/shard_map/all_to_all | solution.py:64
  94.9 5.0 %all-to-all-done.2 = bf16[4,64,256]{2,1,0:T(8,128)(2,1)S(1)} async-done(((bf16[4,64,256]{2,1,0:T(8,128)(2,1)}), bf16[4,64,256]{2,1,0:T(8,128)(2,1)S(1)}, u32[]{:S(2)}, u32[]{:S(2)}) %all-to-all-start.2) | async-done | bytes 131104 | tf_op jit(solution)/shard_map/all_to_all | solution.py:64
  100.0 0.7 gather_fusion
  100.7 0.7 select_convert_fusion
  (5 shorter events, 0.0 us)
Async XLA Ops:
  6.5 43.4 %copy-start = (bf16[4,128,2048]{2,1,0:T(8,128)(2,1)S(1)}, bf16[4,128,2048]{2,1,0:T(8,128)(2,1)}, u32[]{:S(2)}) copy-start(bf16[4,128,2048]{2,1,0:T(8,128)(2,1)} %param.15) | copy-start | bytes 6291460
  6.5 38.3 %all-gather.2.cloned.1.call-start = ((), (), s32[]{:S(2)}) async-start(), calls=%async_computation.4 | async-start | bytes 1179648 | tf_op jit(solution)/shard_map/all_gather | solution.py:46
  20.1 69.1 %reduce-scatter.2.cloned.1.call-start = ((), (), s32[]{:S(2)}) async-start(), calls=%async_computation.5 | async-start | bytes 2359296 | tf_op jit(solution)/shard_map/reduce_scatter | solution.py:11
  46.5 1.9 %copy-start.2 = (bf16[4,128,2048]{2,1,0:T(8,128)(2,1)S(1)}, bf16[4,128,2048]{2,1,0:T(8,128)(2,1)}, u32[]{:S(2)}) copy-start(bf16[4,128,2048]{2,1,0:T(8,128)(2,1)} %param.13) | copy-start | bytes 6291460
  55.2 0.7 copy-start.1
  90.8 9.1 %all-to-all-start.2 = ((bf16[4,64,256]{2,1,0:T(8,128)(2,1)}), bf16[4,64,256]{2,1,0:T(8,128)(2,1)S(1)}, u32[]{:S(2)}, u32[]{:S(2)}) async-start(bf16[4,64,256]{2,1,0:T(8,128)(2,1)} %bitcast.12), calls=%async_computation.3 | async-start | bytes 262144 | tf_op jit(solution)/shard_map/all_to_all | solution.py:64
Sparse Core Ops, SparseCore 0:
  20.2 24.5 all-gather.1
  55.4 33.8 reduce-scatter.1
where the time goes:
time: 109 us; the launch traced here: 108 us
  waiting for transfers between devices  53.5 us (49%)
  blocking collectives  17.2 us (16%)
  between operations  13.4 us (12%)
  other arithmetic  9.38 us (9%)
  matrix products  8.06 us (7%)
  starting transfers between devices  4.15 us (4%)
  local copies, waits for them, and re-layouts  2.42 us (2%)
    reduce_scatter x1, waiting for transfers between devices, scattered(): lax.psum_scatter(portion(jnp.int32(0), count), axis, scatter_dimension=0,...  33.3 us
    all_gather x1, waiting for transfers between devices, per_device(): lax.all_gather(arrived_rows, 'tp', axis=2, tiled=True)  15.2 us
    all_to_all x1, blocking collectives, per_device(): lax.all_to_all(packed_rows, 'ep', split_axis=0, concat_axis=0, tiled=True)  10.2 us
    all_to_all x1, blocking collectives, per_device(): lax.all_to_all(packed_gates, 'ep', split_axis=0, concat_axis=0, tiled=True)  7.05 us
    dot_general x1, matrix products, weighted_sum(): jnp.einsum('esf,efd->esd', hidden, down_part, preferred_element_type=jnp....  5.28 us
    all_to_all x1, waiting for transfers between devices, per_device(): lax.all_to_all(partial_rows.astype(jnp.bfloat16), 'ep', split_axis=0, con...  5.01 us
    all_to_all x1, starting transfers between devices, per_device(): lax.all_to_all(partial_rows.astype(jnp.bfloat16), 'ep', split_axis=0, con...  4.1 us
  transfers between devices with their start and end apart: 3, of which 3 were waited for; matrix products, arithmetic and copies ran while one was open for 2% of the time, Pallas kernels for 0%

commit v1 on v0

--- a/solution.py
+++ b/solution.py
@@ -1,9 +1,304 @@
+import functools
+
 import jax
 import jax.numpy as jnp
 from jax import lax
+from jax.experimental import pallas as pl
+from jax.experimental.pallas import tpu as pltpu
 from jax.sharding import PartitionSpec as P
 
 epsilon = 1e-06
+MESH = pl.DeviceIdType.MESH
+
+
+def fused_kernel(
+    nz,
+    tokens,
+    gain,
+    group_pick,
+    inner_pick,
+    route_weight,
+    wg_hbm,
+    wu_hbm,
+    wd_hbm,
+    out,
+    wg,
+    wu,
+    wd,
+    rows,
+    gates,
+    normed,
+    hcat,
+    to_core,
+    from_core,
+    part_a,
+    part_b,
+    in_a1,
+    in_b1,
+    in_a2,
+    in_b2,
+    fin,
+    in_z,
+    w_sem,
+    row_send,
+    row_recv,
+    gate_send,
+    gate_recv,
+    core_send,
+    core_recv,
+    xy_send,
+    xy_recv,
+    z_send,
+    z_recv,
+):
+    ep, tp = lax.axis_index("ep"), lax.axis_index("tp")
+    z, core = tp // 2, tp % 2
+    twin = (ep, z * 2 + (1 - core))
+    peer = [None, (ep ^ 1, tp), (ep ^ 2, tp), (ep ^ 3, tp)]
+    tok, share = tokens.shape
+    inner = wd_hbm.shape[0]
+    width = wd_hbm.shape[1]
+    half = share // 2
+
+    def at_z(dz):
+        return lax.rem(z + dz, nz)
+
+    loads = [
+        pltpu.make_async_copy(src, dst, w_sem.at[i])
+        for i, (src, dst) in enumerate(((wg_hbm, wg), (wu_hbm, wu), (wd_hbm, wd)))
+    ]
+    for load in loads:
+        load.start()
+
+    barrier = pltpu.get_barrier_semaphore()
+    greeted = [twin] + peer[1:] + [(ep, at_z(dz) * 2 + core) for dz in range(1, nz)]
+    for device in greeted:
+        pl.semaphore_signal(barrier, inc=1, device_id=device, device_id_type=MESH)
+
+    lane = lax.broadcasted_iota(jnp.int32, (tok, 128), 1)
+    relative = (group_pick[...] ^ ep) * inner
+    table = jnp.zeros((tok, 128), jnp.float32)
+    for k in range(inner_pick.shape[1]):
+        key = relative + inner_pick[:, k : k + 1]
+        table = table + jnp.where(lane == key, route_weight[:, k : k + 1], 0.0)
+    table = jnp.concatenate([table, jnp.zeros((128 - tok, 128), jnp.float32)], axis=0)
+    gates[0] = jnp.transpose(table)[: gates.shape[1], :]
+    rows[0, tp] = tokens[...]
+
+    pl.semaphore_wait(barrier, len(greeted))
+
+    sent = []
+
+    def send(src, dst, send_sem, recv_sem, device):
+        copy = pltpu.make_async_remote_copy(
+            src_ref=src,
+            dst_ref=dst,
+            send_sem=send_sem,
+            recv_sem=recv_sem,
+            device_id=device,
+            device_id_type=MESH,
+        )
+        copy.start()
+        sent.append(copy)
+
+    def arrived(dst, recv_sem):
+        pltpu.make_async_remote_copy(
+            src_ref=dst,
+            dst_ref=dst,
+            send_sem=recv_sem,
+            recv_sem=recv_sem,
+            device_id=twin,
+            device_id_type=MESH,
+        ).wait_recv()
+
+    counter = [0]
+
+    def send_row(src, r, t, device):
+        i = counter[0]
+        counter[0] += 1
+        send(src, rows.at[r, t], row_send.at[i], row_recv.at[r, t], device)
+
+    def row_arrived(r, t):
+        arrived(rows.at[r, t], row_recv.at[r, t])
+
+    for dz in range(1, nz):
+        send_row(tokens, 0, tp, (ep, at_z(dz) * 2 + core))
+    send_row(tokens, 1, tp, peer[1])
+    send_row(tokens, 2, tp, peer[2])
+    send_row(tokens, 0, tp, twin)
+    for r in range(1, 4):
+        send(gates.at[0], gates.at[r], gate_send.at[r], gate_recv.at[r], peer[r])
+    order = sorted(range(nz), key=lambda dz: min(dz, nz - dz))
+    for dz in order[1:]:
+        t = at_z(dz) * 2 + core
+        row_arrived(0, t)
+        send_row(rows.at[0, t], 1, t, peer[1])
+        send_row(rows.at[0, t], 2, t, peer[2])
+        send_row(rows.at[0, t], 0, t, twin)
+    for i, dz in enumerate(order):
+        t = at_z(dz) * 2 + core
+        row_arrived(1, t)
+        if i % 2 == 0:
+            send_row(rows.at[1, t], 3, t, peer[2])
+        send_row(rows.at[1, t], 1, t, twin)
+        row_arrived(2, t)
+        if i % 2 == 1:
+            send_row(rows.at[2, t], 3, t, peer[1])
+        send_row(rows.at[2, t], 2, t, twin)
+    for dz in order:
+        t = at_z(dz) * 2 + core
+        row_arrived(3, t)
+        send_row(rows.at[3, t], 3, t, twin)
+
+    columns = []
+    for r in range(4):
+        if r > 0:
+            arrived(gates.at[r], gate_recv.at[r])
+        for dz in range(nz):
+            row_arrived(r, at_z(dz) * 2 + (1 - core))
+        total = jnp.zeros((tok, 1), jnp.float32)
+        for t in range(2 * nz):
+            piece = rows[r, t].astype(jnp.float32)
+            total = total + jnp.sum(piece * piece, axis=1, keepdims=True)
+        scaled = lax.rsqrt(total / (2 * nz * share) + epsilon)
+        for t in range(2 * nz):
+            piece = rows[r, t].astype(jnp.float32)
+            span = slice(t * share, (t + 1) * share)
+            normed[r * tok : (r + 1) * tok, span] = (piece * scaled * gain[:, span]).astype(jnp.bfloat16)
+        turned = jnp.transpose(gates[r])[:tok]
+        columns.append([turned[:, r * inner + e : r * inner + e + 1] for e in range(inner)])
+
+    loads[0].wait()
+    loads[1].wait()
+    count = 4 * tok
+    contract = (((1,), (1,)), ((), ()))
+    for e in range(0, inner, 2):
+        pair = wg[e : e + 2].reshape(2 * width, -1)
+        gate_proj = lax.dot_general(normed[...], pair, contract, preferred_element_type=jnp.float32)
+        pair = wu[e : e + 2].reshape(2 * width, -1)
+        up_proj = lax.dot_general(normed[...], pair, contract, preferred_element_type=jnp.float32)
+        hidden = gate_proj / (1.0 + jnp.exp(-gate_proj)) * up_proj
+        hidden = hidden.astype(jnp.bfloat16).astype(jnp.float32)
+        for j in range(2):
+            weight = jnp.concatenate([columns[r][e + j] for r in range(4)], axis=0)
+            weighted = hidden[:, j * width : (j + 1) * width] * weight
+            high = weighted.astype(jnp.bfloat16)
+            low = (weighted - high.astype(jnp.float32)).astype(jnp.bfloat16)
+            span = slice((e + j) * width, (e + j + 1) * width)
+            hcat[:count, span] = high
+            hcat[count:, span] = low
+
+    loads[2].wait()
+
+    def down(t):
+        cols = pl.ds(pl.multiple_of(t * share, share), share)
+        both = jnp.dot(
+            hcat[...],
+            wd[:, :, cols].reshape(inner * width, share),
+            preferred_element_type=jnp.float32,
+        )
+        return both[:count] + both[count:]
+
+    offsets = sorted(range(1, nz), key=lambda dz: -min(dz, nz - dz)) + [0]
+    for k, dz in enumerate(offsets):
+        to_core[k] = down(at_z(dz) * 2 + (1 - core))
+        send(to_core.at[k], from_core.at[k], core_send.at[k], core_recv.at[k], twin)
+        mine = down(at_z(dz) * 2 + core)
+        arrived(from_core.at[k], core_recv.at[k])
+        for slot in range(4):
+            ra = (0, 2, 1, 3)[slot]
+            part_a[k, slot] = (
+                mine[ra * tok : (ra + 1) * tok, :half] + from_core[k, ra * tok : (ra + 1) * tok, :half]
+            )
+            part_b[k, slot] = (
+                mine[slot * tok : (slot + 1) * tok, half:] + from_core[k, slot * tok : (slot + 1) * tok, half:]
+            )
+        send(part_a.at[k, pl.ds(2, 2)], in_a1.at[k], xy_send.at[k, 0], xy_recv.at[k, 0], peer[1])
+        send(part_b.at[k, pl.ds(2, 2)], in_b1.at[k], xy_send.at[k, 1], xy_recv.at[k, 1], peer[2])
+
+    def second(k):
+        arrived(in_a1.at[k], xy_recv.at[k, 0])
+        part_a[k, 1] += in_a1[k, 1]
+        send(part_a.at[k, 1], in_a2.at[k], xy_send.at[k, 2], xy_recv.at[k, 2], peer[2])
+        arrived(in_b1.at[k], xy_recv.at[k, 1])
+        part_b[k, 1] += in_b1[k, 1]
+        send(part_b.at[k, 1], in_b2.at[k], xy_send.at[k, 3], xy_recv.at[k, 3], peer[1])
+
+    def last(k):
+        arrived(in_a2.at[k], xy_recv.at[k, 2])
+        fin[k, :, :half] = part_a[k, 0] + in_a1[k, 0] + in_a2[k]
+        arrived(in_b2.at[k], xy_recv.at[k, 3])
+        fin[k, :, half:] = part_b[k, 0] + in_b1[k, 0] + in_b2[k]
+        if offsets[k] != 0:
+            device = (ep, at_z(offsets[k]) * 2 + core)
+            send(fin.at[k], in_z.at[k], z_send.at[k], z_recv.at[k], device)
+
+    for k in range(nz):
+        second(k)
+        if k > 0:
+            last(k - 1)
+    last(nz - 1)
+    total = fin[nz - 1]
+    for k in range(nz - 1):
+        arrived(in_z.at[k], z_recv.at[k])
+        total = total + in_z[k]
+    out[...] = total.astype(out.dtype)
+    for copy in sent:
+        copy.wait_send()
+
+
+def fused(tokens, norm_gain, group_pick, inner_pick, route_weight, w_gate, w_up, w_down):
+    tp_size = lax.axis_size("tp")
+    nz = tp_size // 2
+    tok, share = tokens.shape
+    inner, width, features = w_gate.shape
+    half = share // 2
+    count = 4 * tok
+    gate_rows = -(-4 * inner // 8) * 8
+    f32, bf16 = jnp.float32, jnp.bfloat16
+    vmem = pl.BlockSpec(memory_space=pltpu.VMEM)
+    hbm = pl.BlockSpec(memory_space=pl.ANY)
+    dma = pltpu.SemaphoreType.DMA
+    sends = (nz - 1) + 3 + 3 * (nz - 1) + 3 * nz + nz
+    return pl.pallas_call(
+        functools.partial(fused_kernel, nz),
+        out_shape=jax.ShapeDtypeStruct((tok, share), bf16),
+        in_specs=[vmem] * 5 + [hbm] * 3,
+        out_specs=vmem,
+        scratch_shapes=[
+            pltpu.VMEM((inner, width, features), bf16),
+            pltpu.VMEM((inner, width, features), bf16),
+            pltpu.VMEM((inner, width, features), bf16),
+            pltpu.VMEM((4, tp_size, tok, share), bf16),
+            pltpu.VMEM((4, gate_rows, 128), f32),
+            pltpu.VMEM((count, features), bf16),
+            pltpu.VMEM((2 * count, inner * width), bf16),
+            pltpu.VMEM((nz, count, share), f32),
+            pltpu.VMEM((nz, count, share), f32),
+            pltpu.VMEM((nz, 4, tok, half), f32),
+            pltpu.VMEM((nz, 4, tok, half), f32),
+            pltpu.VMEM((nz, 2, tok, half), f32),
+            pltpu.VMEM((nz, 2, tok, half), f32),
+            pltpu.VMEM((nz, tok, half), f32),
+            pltpu.VMEM((nz, tok, half), f32),
+            pltpu.VMEM((nz, tok, share), f32),
+            pltpu.VMEM((nz, tok, share), f32),
+            dma((3,)),
+            dma((sends,)),
+            dma((4, tp_size)),
+            dma((4,)),
+            dma((4,)),
+            dma((nz,)),
+            dma((nz,)),
+            dma((nz, 4)),
+            dma((nz, 4)),
+            dma((nz,)),
+            dma((nz,)),
+        ],
+        compiler_params=pltpu.CompilerParams(
+            collective_id=0, has_side_effects=True, vmem_limit_bytes=48 * 1024 * 1024
+        ),
+    )(tokens, norm_gain.reshape(1, -1), group_pick, inner_pick, route_weight, w_gate, w_up, w_down)
 
 
 def scattered(portion, rows, axis):
@@ -72,8 +367,9 @@
 
 
 def solution(mesh):
+    square = mesh.shape["ep"] == 4 and mesh.shape["tp"] % 2 == 0
     return jax.shard_map(
-        per_device,
+        fused if square else per_device,
         mesh=mesh,
         in_specs=(
             P("ep", "tp"),

time: 109 us -> 46.5 us (0.43)
  waiting for transfers between devices: 53.5 us -> 0 us
  Pallas kernels: 0 us -> 38.6 us
  blocking collectives: 17.2 us -> 0 us
  between operations: 13.4 us -> 0.01 us
  other arithmetic: 9.38 us -> 0 us
  matrix products: 8.06 us -> 0 us
  local copies, waits for them, and re-layouts: 2.42 us -> 7.53 us
  starting transfers between devices: 4.15 us -> 0 us
    pallas_call x0 -> x1, Pallas kernels: none -> 38.6 us  [fused(): pl.pallas_call(functools.partial(fused_kernel, nz), out_shape=jax.ShapeDt...]
    reduce_scatter x1 -> x0, waiting for transfers between devices: 33.3 us -> none  [scattered(): lax.psum_scatter(portion(jnp.int32(0), count), axis, scatter_dimension=0,...]
    all_to_all x2 -> x0, blocking collectives: 17.2 us -> none  [the longest x1 10.2 us: per_device(): lax.all_to_all(packed_rows, 'ep', split_axis=0, concat_axis=0, tiled=True)]
    all_gather x1 -> x0, waiting for transfers between devices: 15.2 us -> none  [per_device(): lax.all_gather(arrived_rows, 'tp', axis=2, tiled=True)]
    dot_general x4 -> x0, matrix products: 8.06 us -> none  [the longest x1 5.28 us: weighted_sum(): jnp.einsum('esf,efd->esd', hidden, down_part, preferred_element_type=jnp....]
    unnamed x8 -> x12, local copies, waits for them, and re-layouts: 1.03 us -> 7.53 us
    all_to_all x1 -> x0, waiting for transfers between devices: 5.01 us -> none  [per_device(): lax.all_to_all(partial_rows.astype(jnp.bfloat16), 'ep', split_axis=0, con...]
    convert_element_type x4 -> x0, other arithmetic: 4.87 us -> none  [the longest x1 1.7 us: rms_normed(): return (widened * scaled * norm_gain).astype(jnp.bfloat16)]
  transfers between devices with their start and end apart: 3 -> 0, of which waited for: 3 -> 0; matrix products, arithmetic and copies ran while one was open for 2% -> 0% of each run, Pallas kernels for 0% -> 0%
where the time goes in v1:
time: 46.5 us; the launch traced here: 46.2 us
  Pallas kernels  38.6 us (83%)
  local copies, waits for them, and re-layouts  7.53 us (16%)
    pallas_call x1, Pallas kernels, fused(): pl.pallas_call(functools.partial(fused_kernel, nz), out_shape=jax.ShapeDt...  38.6 us
    unnamed x12, local copies, waits for them, and re-layouts  7.53 us

profile of v1, /device:TPU:0, one launch (start us, length us, event | category | flops | bytes accessed | tf_op | source)
XLA Modules:
  0.0 46.2 jit_solution(7902479763411582284)
XLA Ops:
  0.0 0.7 %copy.9.group_pick = s32[64,1]{1,0:T(8,128)S(1)} copy(s32[64,1]{0,1:T(1,128)} %param.10) | data formatting | bytes 512 | tf_op args[2]
  0.7 0.8 %copy.10.inner_pick = s32[64,2]{1,0:T(8,128)S(1)} copy(s32[64,2]{0,1:T(2,128)} %param.11) | data formatting | bytes 1024 | tf_op args[3]
  1.5 0.8 %copy.11.route_weight = f32[64,2]{1,0:T(8,128)S(1)} copy(f32[64,2]{0,1:T(2,128)} %param.12) | data formatting | bytes 1024 | tf_op args[4]
  2.3 0.0 copy-start
  2.3 1.6 %copy-done = bf16[4,128,2048]{2,1,0:T(8,128)(2,1)S(1)} copy-done((bf16[4,128,2048]{2,1,0:T(8,128)(2,1)S(1)}, bf16[4,128,2048]{2,1,0:T(8,128)(2,1)}, u32[]{:S(2)}) %copy-start) | copy-done | bytes 2097176
  3.9 0.0 copy-start.1
  3.9 1.6 %copy-done.1 = bf16[4,128,2048]{2,1,0:T(8,128)(2,1)S(1)} copy-done((bf16[4,128,2048]{2,1,0:T(8,128)(2,1)S(1)}, bf16[4,128,2048]{2,1,0:T(8,128)(2,1)}, u32[]{:S(2)}) %copy-start.1) | copy-done | bytes 2097176
  5.5 0.0 copy-start.2
  5.5 0.8 %copy-done.2 = bf16[64,256]{1,0:T(8,128)(2,1)S(1)} copy-done((bf16[64,256]{1,0:T(8,128)(2,1)S(1)}, bf16[64,256]{1,0:T(8,128)(2,1)}, u32[]{:S(2)}) %copy-start.2) | copy-done | bytes 32792
  6.2 0.0 copy-start.3
  6.2 0.7 %copy-done.3 = f32[2048]{0:T(1024)S(1)} copy-done((f32[2048]{0:T(1024)S(1)}, f32[2048]{0:T(1024)}, u32[]{:S(2)}) %copy-start.3) | copy-done | bytes 8216
  6.9 38.6 %shard_map.82 = bf16[64,256]{1,0:T(8,128)(2,1)S(1)} custom-call(bf16[64,256]{1,0:T(8,128)(2,1)S(1)} %copy-done.2, f32[1,2048]{1,0:T(1,128)S(1)} %bitcast.1, s32[64,1]{1,0:T(8,128)S(1)} %copy.9.group_pick, s32[64,2]{1,0:T(8,128)S(1)} %copy.10.inner_pick, f32[64,2]{1,0:T(8,128)S(1)} %copy.11.route_weight, bf16[4,128,2048]{2,1,0:T(8,128)(2,1)S(1)} %copy-done, ...), custom_call_target="tpu_custom_call" | custom-call | tf_op jit(solution)/shard_map/pallas_call | solution.py:263
  45.6 0.6 %copy.13 = bf16[64,256]{1,0:T(8,128)(2,1)} copy(bf16[64,256]{1,0:T(8,128)(2,1)S(1)} %shard_map.82) | data formatting | bytes 65536
Async XLA Ops:
  2.3 1.6 %copy-start = (bf16[4,128,2048]{2,1,0:T(8,128)(2,1)S(1)}, bf16[4,128,2048]{2,1,0:T(8,128)(2,1)}, u32[]{:S(2)}) copy-start(bf16[4,128,2048]{2,1,0:T(8,128)(2,1)} %wg_hbm.1) | copy-start | bytes 6291460
  3.9 1.6 %copy-start.1 = (bf16[4,128,2048]{2,1,0:T(8,128)(2,1)S(1)}, bf16[4,128,2048]{2,1,0:T(8,128)(2,1)}, u32[]{:S(2)}) copy-start(bf16[4,128,2048]{2,1,0:T(8,128)(2,1)} %wu_hbm.1) | copy-start | bytes 6291460
  5.5 0.8 %copy-start.2 = (bf16[64,256]{1,0:T(8,128)(2,1)S(1)}, bf16[64,256]{1,0:T(8,128)(2,1)}, u32[]{:S(2)}) copy-start(bf16[64,256]{1,0:T(8,128)(2,1)} %tokens.1) | copy-start | bytes 98308
  6.2 0.7 %copy-start.3 = (f32[2048]{0:T(1024)S(1)}, f32[2048]{0:T(1024)}, u32[]{:S(2)}) copy-start(f32[2048]{0:T(1024)} %param.9) | copy-start | bytes 24580

commit v2 on v1

--- a/solution.py
+++ b/solution.py
@@ -13,15 +13,20 @@
 
 def fused_kernel(
     nz,
+    tokens_hbm,
+    gain_hbm,
+    group_hbm,
+    inner_hbm,
+    route_hbm,
+    wg_hbm,
+    wu_hbm,
+    wd_hbm,
+    out,
     tokens,
     gain,
     group_pick,
     inner_pick,
     route_weight,
-    wg_hbm,
-    wu_hbm,
-    wd_hbm,
-    out,
     wg,
     wu,
     wd,
@@ -65,7 +70,18 @@
 
     loads = [
         pltpu.make_async_copy(src, dst, w_sem.at[i])
-        for i, (src, dst) in enumerate(((wg_hbm, wg), (wu_hbm, wu), (wd_hbm, wd)))
+        for i, (src, dst) in enumerate(
+            (
+                (tokens_hbm, tokens),
+                (group_hbm, group_pick),
+                (inner_hbm, inner_pick),
+                (route_hbm, route_weight),
+                (gain_hbm, gain),
+                (wg_hbm, wg),
+                (wu_hbm, wu),
+                (wd_hbm, wd),
+            )
+        )
     ]
     for load in loads:
         load.start()
@@ -75,14 +91,16 @@
     for device in greeted:
         pl.semaphore_signal(barrier, inc=1, device_id=device, device_id_type=MESH)
 
-    lane = lax.broadcasted_iota(jnp.int32, (tok, 128), 1)
+    for load in loads[:4]:
+        load.wait()
+    gate_rows = gates.shape[1]
+    row = lax.broadcasted_iota(jnp.int32, (gate_rows, tok), 0)
     relative = (group_pick[...] ^ ep) * inner
-    table = jnp.zeros((tok, 128), jnp.float32)
-    for k in range(inner_pick.shape[1]):
-        key = relative + inner_pick[:, k : k + 1]
-        table = table + jnp.where(lane == key, route_weight[:, k : k + 1], 0.0)
-    table = jnp.concatenate([table, jnp.zeros((128 - tok, 128), jnp.float32)], axis=0)
-    gates[0] = jnp.transpose(table)[: gates.shape[1], :]
+    table = jnp.zeros((gate_rows, tok), jnp.float32)
+    for k in range(inner_pick.shape[0]):
+        key = relative + inner_pick[k : k + 1, :]
+        table = table + jnp.where(row == key, route_weight[k : k + 1, :], 0.0)
+    gates[0] = jnp.concatenate([table, jnp.zeros((gate_rows, 128 - tok), jnp.float32)], axis=1)
     rows[0, tp] = tokens[...]
 
     pl.semaphore_wait(barrier, len(greeted))
@@ -135,23 +153,10 @@
         send_row(rows.at[0, t], 1, t, peer[1])
         send_row(rows.at[0, t], 2, t, peer[2])
         send_row(rows.at[0, t], 0, t, twin)
-    for i, dz in enumerate(order):
-        t = at_z(dz) * 2 + core
-        row_arrived(1, t)
-        if i % 2 == 0:
-            send_row(rows.at[1, t], 3, t, peer[2])
-        send_row(rows.at[1, t], 1, t, twin)
-        row_arrived(2, t)
-        if i % 2 == 1:
-            send_row(rows.at[2, t], 3, t, peer[1])
-        send_row(rows.at[2, t], 2, t, twin)
-    for dz in order:
-        t = at_z(dz) * 2 + core
-        row_arrived(3, t)
-        send_row(rows.at[3, t], 3, t, twin)
 
     columns = []
-    for r in range(4):
+
+    def norm(r):
         if r > 0:
             arrived(gates.at[r], gate_recv.at[r])
         for dz in range(nz):
@@ -168,8 +173,28 @@
         turned = jnp.transpose(gates[r])[:tok]
         columns.append([turned[:, r * inner + e : r * inner + e + 1] for e in range(inner)])
 
-    loads[0].wait()
-    loads[1].wait()
+    loads[4].wait()
+    norm(0)
+    for i, dz in enumerate(order):
+        t = at_z(dz) * 2 + core
+        row_arrived(1, t)
+        if i % 2 == 0:
+            send_row(rows.at[1, t], 3, t, peer[2])
+        send_row(rows.at[1, t], 1, t, twin)
+        row_arrived(2, t)
+        if i % 2 == 1:
+            send_row(rows.at[2, t], 3, t, peer[1])
+        send_row(rows.at[2, t], 2, t, twin)
+    norm(1)
+    norm(2)
+    for dz in order:
+        t = at_z(dz) * 2 + core
+        row_arrived(3, t)
+        send_row(rows.at[3, t], 3, t, twin)
+    norm(3)
+
+    loads[5].wait()
+    loads[6].wait()
     count = 4 * tok
     contract = (((1,), (1,)), ((), ()))
     for e in range(0, inner, 2):
@@ -188,7 +213,7 @@
             hcat[:count, span] = high
             hcat[count:, span] = low
 
-    loads[2].wait()
+    loads[7].wait()
 
     def down(t):
         cols = pl.ds(pl.multiple_of(t * share, share), share)
@@ -253,6 +278,7 @@
     tok, share = tokens.shape
     inner, width, features = w_gate.shape
     half = share // 2
+    top = inner_pick.shape[1]
     count = 4 * tok
     gate_rows = -(-4 * inner // 8) * 8
     f32, bf16 = jnp.float32, jnp.bfloat16
@@ -263,9 +289,14 @@
     return pl.pallas_call(
         functools.partial(fused_kernel, nz),
         out_shape=jax.ShapeDtypeStruct((tok, share), bf16),
-        in_specs=[vmem] * 5 + [hbm] * 3,
+        in_specs=[hbm] * 8,
         out_specs=vmem,
         scratch_shapes=[
+            pltpu.VMEM((tok, share), bf16),
+            pltpu.VMEM((1, features), f32),
+            pltpu.VMEM((1, tok), jnp.int32),
+            pltpu.VMEM((top, tok), jnp.int32),
+            pltpu.VMEM((top, tok), f32),
             pltpu.VMEM((inner, width, features), bf16),
             pltpu.VMEM((inner, width, features), bf16),
             pltpu.VMEM((inner, width, features), bf16),
@@ -283,7 +314,7 @@
             pltpu.VMEM((nz, tok, half), f32),
             pltpu.VMEM((nz, tok, share), f32),
             pltpu.VMEM((nz, tok, share), f32),
-            dma((3,)),
+            dma((8,)),
             dma((sends,)),
             dma((4, tp_size)),
             dma((4,)),
@@ -296,9 +327,18 @@
             dma((nz,)),
         ],
         compiler_params=pltpu.CompilerParams(
-            collective_id=0, has_side_effects=True, vmem_limit_bytes=48 * 1024 * 1024
+            collective_id=0, has_side_effects=True, vmem_limit_bytes=67043328
         ),
-    )(tokens, norm_gain.reshape(1, -1), group_pick, inner_pick, route_weight, w_gate, w_up, w_down)
+    )(
+        tokens,
+        norm_gain.reshape(1, -1),
+        group_pick.T,
+        inner_pick.T,
+        route_weight.T,
+        w_gate,
+        w_up,
+        w_down,
+    )
 
 
 def scattered(portion, rows, axis):

time: 46.5 us -> 40.6 us (0.87)
  local copies, waits for them, and re-layouts: 7.53 us -> 1.38 us
  Pallas kernels: 38.6 us -> 39.1 us
    unnamed x12 -> x1, local copies, waits for them, and re-layouts: 7.53 us -> 1.38 us
where the time goes in v2:
time: 40.6 us; the launch traced here: 40.4 us
  Pallas kernels  39.1 us (96%)
  local copies, waits for them, and re-layouts  1.38 us (3%)
    pallas_call x1, Pallas kernels, fused(): pl.pallas_call(functools.partial(fused_kernel, nz), out_shape=jax.ShapeDt...  39.1 us
    unnamed x1, local copies, waits for them, and re-layouts  1.38 us

profile of v2, /device:TPU:0, one launch (start us, length us, event | category | flops | bytes accessed | tf_op | source)
XLA Modules:
  0.0 40.4 jit_solution(9252045435354227233)
XLA Ops:
  0.0 39.1 %shard_map.82 = bf16[64,256]{1,0:T(8,128)(2,1)} custom-call(bf16[64,256]{1,0:T(8,128)(2,1)} %tokens_hbm.1, f32[1,2048]{1,0:T(1,128)} %bitcast.4, s32[1,64]{1,0:T(1,128)} %bitcast.7, s32[2,64]{1,0:T(2,128)} %bitcast.5, f32[2,64]{1,0:T(2,128)} %bitcast.6, bf16[4,128,2048]{2,1,0:T(8,128)(2,1)} %wg_hbm.1, bf16[4,128,2048]{2,1,0:T(8,128)(2,1)} %wu_hbm.1, ...), custom_call_target="tpu_custom_call" | custom-call | tf_op jit(solution)/shard_map/pallas_call | solution.py:289
  39.1 1.4 %copy.10 = bf16[64,256]{1,0:T(8,128)(2,1)} copy(bf16[64,256]{1,0:T(8,128)(2,1)} %shard_map.82) | data formatting | bytes 65536

commit v3 on v2

--- a/solution.py
+++ b/solution.py
@@ -49,6 +49,8 @@
     row_recv,
     gate_send,
     gate_recv,
+    twin_send,
+    twin_recv,
     core_send,
     core_recv,
     xy_send,
@@ -101,7 +103,8 @@
         key = relative + inner_pick[k : k + 1, :]
         table = table + jnp.where(row == key, route_weight[k : k + 1, :], 0.0)
     gates[0] = jnp.concatenate([table, jnp.zeros((gate_rows, 128 - tok), jnp.float32)], axis=1)
-    rows[0, tp] = tokens[...]
+    own = core * nz + z
+    rows[0, own] = tokens[...]
 
     pl.semaphore_wait(barrier, len(greeted))
 
@@ -140,57 +143,60 @@
         arrived(rows.at[r, t], row_recv.at[r, t])
 
     for dz in range(1, nz):
-        send_row(tokens, 0, tp, (ep, at_z(dz) * 2 + core))
-    send_row(tokens, 1, tp, peer[1])
-    send_row(tokens, 2, tp, peer[2])
-    send_row(tokens, 0, tp, twin)
+        send_row(tokens, 0, own, (ep, at_z(dz) * 2 + core))
+    send_row(tokens, 1, own, peer[1])
+    send_row(tokens, 2, own, peer[2])
+
+    def share_rows(r):
+        mine = rows.at[r, pl.ds(core * nz, nz)]
+        send(mine, mine, twin_send.at[r], twin_recv.at[r], twin)
+
     for r in range(1, 4):
         send(gates.at[0], gates.at[r], gate_send.at[r], gate_recv.at[r], peer[r])
     order = sorted(range(nz), key=lambda dz: min(dz, nz - dz))
     for dz in order[1:]:
-        t = at_z(dz) * 2 + core
+        t = core * nz + at_z(dz)
         row_arrived(0, t)
         send_row(rows.at[0, t], 1, t, peer[1])
         send_row(rows.at[0, t], 2, t, peer[2])
-        send_row(rows.at[0, t], 0, t, twin)
 
     columns = []
 
     def norm(r):
         if r > 0:
             arrived(gates.at[r], gate_recv.at[r])
-        for dz in range(nz):
-            row_arrived(r, at_z(dz) * 2 + (1 - core))
+        arrived(rows.at[r, pl.ds((1 - core) * nz, nz)], twin_recv.at[r])
         total = jnp.zeros((tok, 1), jnp.float32)
         for t in range(2 * nz):
-            piece = rows[r, t].astype(jnp.float32)
+            piece = rows[r, (t % 2) * nz + t // 2].astype(jnp.float32)
             total = total + jnp.sum(piece * piece, axis=1, keepdims=True)
         scaled = lax.rsqrt(total / (2 * nz * share) + epsilon)
         for t in range(2 * nz):
-            piece = rows[r, t].astype(jnp.float32)
+            piece = rows[r, (t % 2) * nz + t // 2].astype(jnp.float32)
             span = slice(t * share, (t + 1) * share)
             normed[r * tok : (r + 1) * tok, span] = (piece * scaled * gain[:, span]).astype(jnp.bfloat16)
         turned = jnp.transpose(gates[r])[:tok]
         columns.append([turned[:, r * inner + e : r * inner + e + 1] for e in range(inner)])
 
+    share_rows(0)
     loads[4].wait()
     norm(0)
     for i, dz in enumerate(order):
-        t = at_z(dz) * 2 + core
+        t = core * nz + at_z(dz)
         row_arrived(1, t)
         if i % 2 == 0:
             send_row(rows.at[1, t], 3, t, peer[2])
-        send_row(rows.at[1, t], 1, t, twin)
         row_arrived(2, t)
         if i % 2 == 1:
             send_row(rows.at[2, t], 3, t, peer[1])
-        send_row(rows.at[2, t], 2, t, twin)
+    share_rows(1)
+    share_rows(2)
     norm(1)
     norm(2)
     for dz in order:
-        t = at_z(dz) * 2 + core
+        t = core * nz + at_z(dz)
         row_arrived(3, t)
-        send_row(rows.at[3, t], 3, t, twin)
+    share_rows(3)
     norm(3)
 
     loads[5].wait()
@@ -225,7 +231,9 @@
         return both[:count] + both[count:]
 
     offsets = sorted(range(1, nz), key=lambda dz: -min(dz, nz - dz)) + [0]
-    for k, dz in enumerate(offsets):
+
+    def first(k):
+        dz = offsets[k]
         to_core[k] = down(at_z(dz) * 2 + (1 - core))
         send(to_core.at[k], from_core.at[k], core_send.at[k], core_recv.at[k], twin)
         mine = down(at_z(dz) * 2 + core)
@@ -258,11 +266,13 @@
             device = (ep, at_z(offsets[k]) * 2 + core)
             send(fin.at[k], in_z.at[k], z_send.at[k], z_recv.at[k], device)
 
-    for k in range(nz):
-        second(k)
-        if k > 0:
-            last(k - 1)
-    last(nz - 1)
+    for k in range(nz + 3):
+        if k < nz:
+            first(k)
+        if 0 <= k - 1 < nz:
+            second(k - 1)
+        if 0 <= k - 2 < nz:
+            last(k - 2)
     total = fin[nz - 1]
     for k in range(nz - 1):
         arrived(in_z.at[k], z_recv.at[k])
@@ -285,7 +295,7 @@
     vmem = pl.BlockSpec(memory_space=pltpu.VMEM)
     hbm = pl.BlockSpec(memory_space=pl.ANY)
     dma = pltpu.SemaphoreType.DMA
-    sends = (nz - 1) + 3 + 3 * (nz - 1) + 3 * nz + nz
+    sends = (nz - 1) + 2 + 2 * (nz - 1) + nz
     return pl.pallas_call(
         functools.partial(fused_kernel, nz),
         out_shape=jax.ShapeDtypeStruct((tok, share), bf16),
@@ -319,6 +329,8 @@
             dma((4, tp_size)),
             dma((4,)),
             dma((4,)),
+            dma((4,)),
+            dma((4,)),
             dma((nz,)),
             dma((nz,)),
             dma((nz, 4)),

time: 40.6 us -> 39.4 us (0.970)
  Pallas kernels: 39.1 us -> 37.8 us
    pallas_call x1, Pallas kernels: 39.1 us -> 37.8 us  [fused(): pl.pallas_call(functools.partial(fused_kernel, nz), out_shape=jax.ShapeDt...]
where the time goes in v3:
time: 39.4 us; the launch traced here: 39.2 us
  Pallas kernels  37.8 us (96%)
  local copies, waits for them, and re-layouts  1.38 us (4%)
    pallas_call x1, Pallas kernels, fused(): pl.pallas_call(functools.partial(fused_kernel, nz), out_shape=jax.ShapeDt...  37.8 us
    unnamed x1, local copies, waits for them, and re-layouts  1.38 us

profile of v3, /device:TPU:0, one launch (start us, length us, event | category | flops | bytes accessed | tf_op | source)
XLA Modules:
  0.0 39.2 jit_solution(10750384749820809343)
XLA Ops:
  0.0 37.8 %shard_map.82 = bf16[64,256]{1,0:T(8,128)(2,1)} custom-call(bf16[64,256]{1,0:T(8,128)(2,1)} %tokens_hbm.1, f32[1,2048]{1,0:T(1,128)} %bitcast.4, s32[1,64]{1,0:T(1,128)} %bitcast.7, s32[2,64]{1,0:T(2,128)} %bitcast.5, f32[2,64]{1,0:T(2,128)} %bitcast.6, bf16[4,128,2048]{2,1,0:T(8,128)(2,1)} %wg_hbm.1, bf16[4,128,2048]{2,1,0:T(8,128)(2,1)} %wu_hbm.1, ...), custom_call_target="tpu_custom_call" | custom-call | tf_op jit(solution)/shard_map/pallas_call | solution.py:299
  37.8 1.4 %copy.10 = bf16[64,256]{1,0:T(8,128)(2,1)} copy(bf16[64,256]{1,0:T(8,128)(2,1)} %shard_map.82) | data formatting | bytes 65536
